TPU v7x, 32 devices: a whole 2x2x4 slice. The times are simulated.
32 devices in a mesh: dp: 2 (over x), kv: 8 (over z, y), tp: 2 (over core).
Axes of the slice: x: 2, y: 2, z: 4, core: 2. Of those that a mesh axis runs over, the one named last changes fastest.
Arguments:
- tokens: bfloat16 [4096, 2048], P(('dp', 'kv')), parts along dimension 0, may hold values from -6 to 6
- query_weight: bfloat16 [2048, 1024], P(None, 'tp'), as said below
- key_weight: bfloat16 [2048, 128], replicated, as said below
- value_weight: bfloat16 [2048, 128], replicated, may hold values from -0.125 to 0.125
- gate_weight: bfloat16 [2048, 32], replicated, may hold values from -0.125 to 0.125
- key_inner: bfloat16 [2048, 64], replicated, as said below
- key_outer: bfloat16 [64, 64], replicated, as said below
- value_inner: bfloat16 [2048, 64], replicated, may hold values from -0.125 to 0.125
- value_outer: bfloat16 [64, 64], replicated, may hold values from -0.75 to 0.75
- out_weight: bfloat16 [1024, 2048], P(None, 'tp'), may hold values from -0.75 to 0.75
- selection: int32 [2, 64, 8], P('tp', ('dp', 'kv')), parts along dimension 1, may hold values from -1 to 31, as said below
Outputs:
- mixed_out: bfloat16 [4096, 2048], P(('dp', 'kv'), 'tp'), parts along dimension 0
There are 2 independent parts, one for each index of `dp`. A program takes and returns all parts, laid end to end along the dimension named above; an argument that names none is the same for every part. Nothing has to cross between parts.
Inputs may be any that keep to these rules, and one draw needn't show every extreme that they name: Slot 0 of selection[g, b] is block b itself; the other slots name distinct blocks before b, or -1 where fewer than 7 blocks lie before b. `query_weight`: every entry lies within six over the square root of 2048 of zero. `key_weight`: every entry lies within six over the square root of 2048 of zero. `key_inner`: every entry lies within six over the square root of 2048 of zero. `key_outer`: every entry lies within six over the square root of 64 of zero.
All inputs are finite; a program needn't handle non-finite values.
Results may differ from a plain program's by a relative error of at most 0.0093.
Values may be sent and summed in bfloat16 or wider, within the bound.
A program may use at most 64 MiB of HBM per device.

v0:
```python
import functools

import jax
import jax.numpy as jnp
from jax import lax
from jax.experimental import pallas as pl
from jax.experimental.pallas import tpu as pltpu
from jax.sharding import PartitionSpec as P

HEAD_DIM = 64
BLOCK = 64
SPAN = 32
LANES = 128
MESH = pl.DeviceIdType.MESH
F32 = jnp.float32
BF16 = jnp.bfloat16
CHUNKS = 4
PARTS = 2


def dot(a, b):
    return jnp.dot(a, b, preferred_element_type=F32)


def dot_t(a, b):
    return lax.dot_general(a, b, (((1,), (1,)), ((), ())), preferred_element_type=F32)


def low_half(shape):
    return lax.broadcasted_iota(jnp.int32, shape, len(shape) - 1) < HEAD_DIM


def kernel(
    n_kv,
    inner,
    sel_ref,
    tok_hbm,
    qw_hbm,
    kw_hbm,
    vw_hbm,
    gw_hbm,
    kin_hbm,
    kout_hbm,
    vin_hbm,
    vout_hbm,
    ow_hbm,
    out_ref,
    tok,
    qw,
    kvw,
    gw,
    kin,
    kout,
    vin,
    vout,
    ow,
    rows32,
    gathered,
    sums,
    stacked,
    summary_mix,
    gate_wide,
    own_mix,
    peer_mix,
    load_sem,
    send_z,
    recv_z,
    send_y,
    recv_y,
    send_s,
    recv_s,
    send_m,
    recv_m,
):
    local, width = tok.shape
    runs = local // SPAN
    blocks = local // BLOCK
    cols = qw.shape[1]
    heads = cols // HEAD_DIM
    pairs = cols // LANES
    picks = sel_ref.shape[2]
    outer = n_kv // inner
    me = lax.axis_index("kv")
    g = lax.axis_index("tp")
    z = me // inner
    y = lax.rem(me, inner)

    depth = width // CHUNKS
    first = []
    for c in range(CHUNKS):
        part = pl.ds(c * depth, depth)
        trio = [
            pltpu.make_async_copy(tok_hbm.at[:, part], tok.at[:, part], load_sem.at[3 * c]),
            pltpu.make_async_copy(
                kw_hbm.at[part], kvw.at[part, pl.ds(0, LANES)], load_sem.at[3 * c + 1]
            ),
            pltpu.make_async_copy(
                vw_hbm.at[part], kvw.at[part, pl.ds(LANES, LANES)], load_sem.at[3 * c + 2]
            ),
        ]
        for copy in trio:
            copy.start()
        first.append(trio)
    base = 3 * CHUNKS
    later = [
        pltpu.make_async_copy(src, dst, load_sem.at[base + i])
        for i, (src, dst) in enumerate(
            [
                (kin_hbm, kin),
                (vin_hbm, vin),
                (kout_hbm, kout),
                (vout_hbm, vout),
                (qw_hbm, qw),
                (gw_hbm, gw),
                (ow_hbm, ow),
            ]
        )
    ]
    kin_c, vin_c, kout_c, vout_c, qw_c, gw_c, ow_c = later

    sums[...] = jnp.zeros_like(sums)
    barrier = pltpu.get_barrier_semaphore()

    def greet(step, carry):
        peer = lax.rem(me + step, n_kv)
        pl.semaphore_signal(barrier, inc=1, device_id={"kv": peer}, device_id_type=MESH)
        return carry

    lax.fori_loop(1, n_kv, greet, 0)
    pl.semaphore_signal(barrier, inc=1, device_id={"tp": 1 - g}, device_id_type=MESH)

    acc = jnp.zeros((local, 2 * LANES), F32)
    for c in range(CHUNKS):
        for copy in first[c]:
            copy.wait()
        if c == CHUNKS - 2:
            for copy in later:
                copy.start()
        part = pl.ds(c * depth, depth)
        acc += dot(tok[:, part], kvw[part, :])
    keys = acc[:, :LANES]
    values = acc[:, LANES:]
    low = low_half((local, LANES))
    paired = jnp.where(
        g == 0,
        jnp.where(low, keys, pltpu.roll(values, HEAD_DIM, 1)),
        jnp.where(low, pltpu.roll(keys, HEAD_DIM, 1), values),
    ).astype(BF16)
    gathered[pl.ds(me * blocks, blocks)] = paired.reshape(blocks, BLOCK, LANES)
    rows32[...] = paired.astype(F32)
    pl.semaphore_wait(barrier, n_kv)

    part_blocks = blocks // PARTS

    def slot(index, part):
        return gathered.at[pl.ds(index * blocks + part * part_blocks, part_blocks)]

    def z_copy(source_z, target_z, part):
        return pltpu.make_async_remote_copy(
            src_ref=slot(source_z * inner + y, part),
            dst_ref=slot(source_z * inner + y, part),
            send_sem=send_z.at[target_z, part],
            recv_sem=recv_z.at[source_z, part],
            device_id={"kv": target_z * inner + y},
            device_id_type=MESH,
        )

    def y_copy(source_z, source_y, step, part):
        return pltpu.make_async_remote_copy(
            src_ref=slot(source_z * inner + source_y, part),
            dst_ref=slot(source_z * inner + source_y, part),
            send_sem=send_y.at[source_z, part],
            recv_sem=recv_y.at[source_z, part],
            device_id={"kv": z * inner + lax.rem(y + step, inner)},
            device_id_type=MESH,
        )

    odd = lax.rem(z, 2)

    def z_send(step, carry):
        target = odd * (z + step) + (1 - odd) * (outer - step)
        for part in range(PARTS):
            z_copy(z, target, part).start()
        return carry

    lax.fori_loop(1, outer - z, z_send, 0)
    if inner == 2:

        @pl.when(y == 0)
        def _():
            for part in range(PARTS):
                y_copy(z, 0, 1, part).start()

    steps = [rows32[pl.ds(j, runs, stride=SPAN), :] for j in range(SPAN)]
    low8 = low_half((runs, LANES))
    flat_k = jnp.concatenate(
        [
            jnp.where(low8, steps[j], pltpu.roll(steps[j + 1], HEAD_DIM, 1))
            for j in range(0, SPAN, 2)
        ],
        axis=1,
    ).astype(BF16)
    flat_v = jnp.concatenate(
        [
            jnp.where(low8, pltpu.roll(steps[j], HEAD_DIM, 1), steps[j + 1])
            for j in range(0, SPAN, 2)
        ],
        axis=1,
    ).astype(BF16)
    kin_c.wait()
    vin_c.wait()
    kout_c.wait()
    vout_c.wait()
    hidden_k = jax.nn.gelu(dot_t(flat_k, kin[...])).astype(BF16)
    hidden_v = jax.nn.gelu(dot_t(flat_v, vin[...])).astype(BF16)
    sum_k = dot(hidden_k, kout[...]).astype(BF16).astype(F32)
    sum_v = dot(hidden_v, vout[...]).astype(BF16).astype(F32)

    def sum_slot(index):
        return sums.at[pl.ds(pl.multiple_of(index * runs, runs), runs), :]

    sums[pl.ds(pl.multiple_of(me * runs, runs), runs), :] = jnp.concatenate([sum_k, sum_v], axis=1)

    def sum_copy(source, target):
        return pltpu.make_async_remote_copy(
            src_ref=sum_slot(source),
            dst_ref=sum_slot(source),
            send_sem=send_s.at[target],
            recv_sem=recv_s.at[source],
            device_id={"kv": target},
            device_id_type=MESH,
        )

    def sum_send(target, carry):
        sum_copy(me, target).start()
        return carry

    lax.fori_loop(me + 1, n_kv, sum_send, 0)

    qw_c.wait()
    queries = dot(tok[...], qw[...]).astype(BF16).astype(F32) * HEAD_DIM**-0.5
    low64 = low_half((BLOCK, LANES))
    for b in range(blocks):
        rows = slice(b * BLOCK, (b + 1) * BLOCK)
        for p in range(pairs):
            two = queries[rows, p * LANES : (p + 1) * LANES]
            at = 2 * p * BLOCK
            stacked[b, at : at + BLOCK] = jnp.where(low64, two, 0.0).astype(BF16)
            stacked[b, at + BLOCK : at + 2 * BLOCK] = jnp.where(
                low64, pltpu.roll(two, HEAD_DIM, 1), 0.0
            ).astype(BF16)
    gw_c.wait()
    gates = jax.nn.sigmoid(dot_t(tok[...], gw[...]))
    half = gates.shape[1] // 2
    gate_s = jnp.where(g == 0, gates[:, :heads], gates[:, heads:half])
    gate_c = jnp.where(g == 0, gates[:, half : half + heads], gates[:, half + heads :])
    for b in range(blocks):
        rows = slice(b * BLOCK, (b + 1) * BLOCK)
        for h in range(heads):
            at = slice(h * BLOCK, (h + 1) * BLOCK)
            gate_wide[b, at] = jnp.broadcast_to(gate_c[rows, h : h + 1], (BLOCK, LANES))
            summary_mix[b, at] = jnp.broadcast_to(gate_s[rows, h : h + 1], (BLOCK, LANES))

    def forward(step, carry):
        is_first = jnp.int32(step == 1)
        source = is_first * (z - 1) + (1 - is_first) * (step - 2)
        for part in range(PARTS):
            z_copy(source, z, part).wait_recv()
            if inner == 2:
                y_copy(source, y, 1, part).start()
        return carry

    lax.fori_loop(1, z + 1, forward, 0)

    def sum_wait(source, carry):
        sum_copy(source, me).wait_recv()
        return carry

    lax.fori_loop(0, me, sum_wait, 0)
    sums_kv = sums[...].astype(BF16)
    total_runs = sums_kv.shape[0]
    sums_kv1 = jnp.concatenate([sums_kv, jnp.ones_like(sums_kv)], axis=1)
    tall = heads * BLOCK
    row_in = lax.rem(lax.broadcasted_iota(jnp.int32, (tall, 1), 0), BLOCK)
    run_end = lax.broadcasted_iota(jnp.int32, (1, total_runs), 1) * SPAN + SPAN - 1
    for b in range(blocks):
        allowed = run_end <= me * local + b * BLOCK + row_in
        shifted = jnp.where(allowed, dot_t(stacked[b], sums_kv), -1e30)
        top = jnp.max(shifted, axis=1, keepdims=True)
        weights = jnp.where(allowed, jnp.exp(shifted - top), 0.0).astype(BF16)
        o_s = dot(weights, sums_kv1)
        summary_mix[b] = summary_mix[b] * o_s[:, :LANES] / jnp.maximum(o_s[:, LANES:], 1.0)

    ow_c.wait()
    if inner == 2:

        def y_wait(step, carry):
            for part in range(PARTS):
                y_copy(z - step, 1 - y, 1, part).wait_recv()
            return carry

        lax.fori_loop(1 - y, z + 1, y_wait, 0)

    lane = lax.broadcasted_iota(jnp.int32, (1, LANES), 1)
    own_allowed = (lane <= row_in) | (lane >= BLOCK)
    mixes = []
    for b in range(blocks):
        rows = slice(b * BLOCK, (b + 1) * BLOCK)
        chosen = [sel_ref[0, b, s] for s in range(picks)]
        kv = jnp.concatenate([gathered[jnp.maximum(c, 0)] for c in chosen], axis=0)
        absent = jnp.concatenate(
            [
                jnp.where(jnp.full((1, BLOCK), c, jnp.int32) >= 0, 0.0, -1e30).astype(F32)
                for c in chosen
            ],
            axis=1,
        )
        scores = dot_t(stacked[b], kv) + absent
        scores = jnp.concatenate(
            [jnp.where(own_allowed, scores[:, :LANES], -1e30), scores[:, LANES:]], axis=1
        )
        top = jnp.max(scores, axis=1, keepdims=True)
        weights = jnp.exp(scores - top).astype(BF16)
        o_c = dot(weights, jnp.concatenate([kv, jnp.ones_like(kv)], axis=1))
        mixed = summary_mix[b] + gate_wide[b] * o_c[:, :LANES] / o_c[:, LANES:]
        for p in range(pairs):
            even = mixed[2 * p * BLOCK : (2 * p + 1) * BLOCK]
            odd_head = mixed[(2 * p + 1) * BLOCK : (2 * p + 2) * BLOCK]
            own_mix[rows, p * LANES : (p + 1) * LANES] = jnp.where(
                low64, pltpu.roll(even, HEAD_DIM, 1), odd_head
            ).astype(BF16)
        mix = pltpu.make_async_remote_copy(
            src_ref=own_mix.at[rows],
            dst_ref=peer_mix.at[rows],
            send_sem=send_m.at[b],
            recv_sem=recv_m.at[b],
            device_id={"tp": 1 - g},
            device_id_type=MESH,
        )
        mix.start()
        mixes.append(mix)

    own_rows = pl.ds(pl.multiple_of(g * cols, cols), cols)
    peer_rows = pl.ds(pl.multiple_of((1 - g) * cols, cols), cols)
    result = dot(own_mix[...], ow[own_rows, :])
    for mix in mixes:
        mix.wait_recv()
    out_ref[...] = (result + dot(peer_mix[...], ow[peer_rows, :])).astype(BF16)
    for mix in mixes:
        mix.wait_send()

    def z_done(step, carry):
        for part in range(PARTS):
            z_copy(z, outer - step, part).wait_send()
        return carry

    lax.fori_loop(1, outer - z, z_done, 0)

    def sum_done(target, carry):
        sum_copy(me, target).wait_send()
        return carry

    lax.fori_loop(me + 1, n_kv, sum_done, 0)
    if inner == 2:

        def y_done(step, carry):
            for part in range(PARTS):
                y_copy(z - step, y, 1, part).wait_send()
            return carry

        lax.fori_loop(y, z + 1, y_done, 0)


def per_device(n_kv, tokens, qw, kw, vw, gw, kin, kout, vin, vout, ow, selection):
    gw, kin, vin = gw.T, kin.T, vin.T
    local, width = tokens.shape
    cols = qw.shape[1]
    inner = 2 if n_kv % 2 == 0 else 1
    outer = n_kv // inner
    blocks = local // BLOCK
    runs = local // SPAN
    tall = cols // HEAD_DIM * BLOCK
    hbm = pl.BlockSpec(memory_space=pltpu.HBM)
    dma = pltpu.SemaphoreType.DMA
    vm = pltpu.VMEM
    return pl.pallas_call(
        functools.partial(kernel, n_kv, inner),
        out_shape=jax.ShapeDtypeStruct((local, ow.shape[1]), BF16),
        in_specs=[pl.BlockSpec(memory_space=pltpu.SMEM)] + [hbm] * 10,
        out_specs=pl.BlockSpec(memory_space=pltpu.VMEM),
        scratch_shapes=[
            vm(tokens.shape, BF16),
            vm(qw.shape, BF16),
            vm((width, 2 * LANES), BF16),
            vm(gw.shape, BF16),
            vm(kin.shape, BF16),
            vm(kout.shape, BF16),
            vm(vin.shape, BF16),
            vm(vout.shape, BF16),
            vm(ow.shape, BF16),
            vm((local, LANES), F32),
            vm((n_kv * blocks, BLOCK, LANES), BF16),
            vm((n_kv * runs, LANES), F32),
            vm((blocks, tall, LANES), BF16),
            vm((blocks, tall, LANES), F32),
            vm((blocks, tall, LANES), F32),
            vm((local, cols), BF16),
            vm((local, cols), BF16),
            dma((3 * CHUNKS + 7,)),
            dma((outer, PARTS)),
            dma((outer, PARTS)),
            dma((outer, PARTS)),
            dma((outer, PARTS)),
            dma((n_kv,)),
            dma((n_kv,)),
            dma((blocks,)),
            dma((blocks,)),
        ],
        compiler_params=pltpu.CompilerParams(collective_id=0, has_side_effects=True),
        name="attend",
    )(selection, tokens, qw, kw, vw, gw, kin, kout, vin, vout, ow)


def solution(mesh):
    in_specs = (
        P(("dp", "kv"), None),
        P(None, "tp"),
        P(),
        P(),
        P(),
        P(),
        P(),
        P(),
        P(),
        P(None, "tp"),
        P("tp", ("dp", "kv"), None),
    )
    out_specs = P(("dp", "kv"), "tp")
    return jax.shard_map(
        functools.partial(per_device, mesh.shape["kv"]),
        mesh=mesh,
        in_specs=in_specs,
        out_specs=out_specs,
        check_vma=False,
    )
```

profile of v0, /device:TPU:25, one launch (start us, length us, event | category | flops | bytes accessed | tf_op | source)
XLA Modules:
  0.0 22.7 jit_solution(4917477767661263982)
XLA Ops:
  0.0 20.8 %attend.1 = bf16[256,1024]{1,0:T(8,128)(2,1)} custom-call(s32[1,4,8]{2,1,0:T(4,128)} %sel_ref.1, bf16[256,2048]{1,0:T(8,128)(2,1)} %tok_hbm.1, bf16[2048,512]{1,0:T(8,128)(2,1)} %qw_hbm.1, bf16[2048,128]{1,0:T(8,128)(2,1)} %kw_hbm.1, bf16[2048,128]{1,0:T(8,128)(2,1)} %vw_hbm.1, bf16[32,2048]{1,0:T(8,128)(2,1)} %bitcast.5, bf16[64,2048]{1,0:T(8,128)(2,1)} %bitcast.3, ...), custom_call_target="tpu_custom_call" | custom-call | tf_op jit(solution)/shard_map/attend/pallas_call | solution.py:386
  20.8 1.9 %copy.13 = bf16[256,1024]{1,0:T(8,128)(2,1)} copy(bf16[256,1024]{1,0:T(8,128)(2,1)} %attend.1) | data formatting | bytes 1048576
where the time goes:
time: 22.9 us; the launch traced here: 22.7 us
  Pallas kernels  20.8 us (91%)
  local copies, waits for them, and re-layouts  1.87 us (8%)
    pallas_call x1, Pallas kernels, per_device(): pl.pallas_call(functools.partial(kernel, n_kv, inner), out_shape=jax.Shap...  20.8 us
    unnamed x1, local copies, waits for them, and re-layouts  1.87 us

commit v1 on v0

v1 whole, which is shorter than its diff:
```python
import functools

import jax
import jax.numpy as jnp
from jax import lax
from jax.experimental import pallas as pl
from jax.experimental.pallas import tpu as pltpu
from jax.sharding import PartitionSpec as P

HEAD_DIM = 64
BLOCK = 64
SPAN = 32
LANES = 128
MESH = pl.DeviceIdType.MESH
F32 = jnp.float32
BF16 = jnp.bfloat16
CHUNKS = 4
PARTS = 2
LOG2E = 1.4426950408889634
GRANT = 40 * 1024 * 1024


def dot(a, b):
    return jnp.dot(a, b, preferred_element_type=F32)


def dot_t(a, b):
    return lax.dot_general(a, b, (((1,), (1,)), ((), ())), preferred_element_type=F32)


def dot_rows(a, b):
    return lax.dot_general(a, b, (((0,), (0,)), ((), ())), preferred_element_type=F32)


def low_half(shape):
    return lax.broadcasted_iota(jnp.int32, shape, len(shape) - 1) < HEAD_DIM


def kernel(
    n_kv,
    inner,
    sel_hbm,
    tok_hbm,
    qw_hbm,
    kw_hbm,
    vw_hbm,
    gw_hbm,
    kin_hbm,
    kout_hbm,
    vin_hbm,
    vout_hbm,
    ow_hbm,
    out_ref,
    sel,
    tok,
    qw,
    kvw,
    gw,
    kin,
    kout,
    vin,
    vout,
    ow,
    rows32,
    gathered,
    sums,
    stacked,
    summary_mix,
    gate_rows,
    own_mix,
    peer_mix,
    partial,
    load_sem,
    ready,
    send_z,
    recv_z,
    send_y,
    recv_y,
    send_s,
    recv_s,
    send_m,
    recv_m,
):
    local, width = tok.shape
    runs = local // SPAN
    blocks = local // BLOCK
    cols = qw.shape[1]
    heads = cols // HEAD_DIM
    pairs = cols // LANES
    picks = sel.shape[2]
    outer = n_kv // inner
    me = lax.axis_index("kv")
    g = lax.axis_index("tp")
    z = me // inner
    y = lax.rem(me, inner)

    barrier = pltpu.get_barrier_semaphore()

    def greet(target, carry):
        pl.semaphore_signal(barrier, inc=1, device_id={"kv": target}, device_id_type=MESH)
        return carry

    lax.fori_loop(me + 1, n_kv, greet, 0)
    pl.semaphore_signal(barrier, inc=1, device_id={"tp": 1 - g}, device_id_type=MESH)

    depth = width // CHUNKS
    first = []
    for c in range(CHUNKS):
        part = pl.ds(c * depth, depth)
        trio = [
            pltpu.make_async_copy(tok_hbm.at[:, part], tok.at[:, part], load_sem.at[3 * c]),
            pltpu.make_async_copy(
                kw_hbm.at[part], kvw.at[part, pl.ds(0, LANES)], load_sem.at[3 * c + 1]
            ),
            pltpu.make_async_copy(
                vw_hbm.at[part], kvw.at[part, pl.ds(LANES, LANES)], load_sem.at[3 * c + 2]
            ),
        ]
        for copy in trio:
            copy.start()
        first.append(trio)
    base = 3 * CHUNKS
    later = [
        pltpu.make_async_copy(src, dst, load_sem.at[base + i])
        for i, (src, dst) in enumerate(
            [
                (kin_hbm, kin),
                (vin_hbm, vin),
                (kout_hbm, kout),
                (vout_hbm, vout),
                (qw_hbm, qw),
                (gw_hbm, gw),
                (sel_hbm, sel),
                (ow_hbm, ow),
            ]
        )
    ]
    kin_c, vin_c, kout_c, vout_c, qw_c, gw_c, sel_c, ow_c = later

    sums[...] = jnp.zeros_like(sums)
    pl.semaphore_wait(barrier, me + 1)

    def tell(target, carry):
        pl.semaphore_signal(ready.at[me], inc=1, device_id={"kv": target}, device_id_type=MESH)
        return carry

    lax.fori_loop(0, me, tell, 0)

    acc = jnp.zeros((local, 2 * LANES), F32)
    for c in range(CHUNKS):
        for copy in first[c]:
            copy.wait()
        if c == CHUNKS - 2:
            for copy in later:
                copy.start()
        part = pl.ds(c * depth, depth)
        acc += dot(tok[:, part], kvw[part, :])
    keys = acc[:, :LANES]
    values = acc[:, LANES:]
    low = low_half((local, LANES))
    paired = jnp.where(
        g == 0,
        jnp.where(low, keys, pltpu.roll(values, HEAD_DIM, 1)),
        jnp.where(low, pltpu.roll(keys, HEAD_DIM, 1), values),
    ).astype(BF16)
    gathered[pl.ds(me * blocks, blocks)] = paired.reshape(blocks, BLOCK, LANES)
    rows32[...] = paired.astype(F32)

    part_blocks = blocks // PARTS

    def slot(index, part):
        return gathered.at[pl.ds(index * blocks + part * part_blocks, part_blocks)]

    def z_copy(source_z, target_z, part):
        return pltpu.make_async_remote_copy(
            src_ref=slot(source_z * inner + y, part),
            dst_ref=slot(source_z * inner + y, part),
            send_sem=send_z.at[target_z, part],
            recv_sem=recv_z.at[source_z, part],
            device_id={"kv": target_z * inner + y},
            device_id_type=MESH,
        )

    def y_copy(source_z, source_y, part):
        return pltpu.make_async_remote_copy(
            src_ref=slot(source_z * inner + source_y, part),
            dst_ref=slot(source_z * inner + source_y, part),
            send_sem=send_y.at[source_z, part],
            recv_sem=recv_y.at[source_z, part],
            device_id={"kv": z * inner + lax.rem(y + 1, inner)},
            device_id_type=MESH,
        )

    def wait_ready(index):
        pl.semaphore_wait(ready.at[index], 1)

    def z_send(target, carry):
        wait_ready(target * inner + y)
        for part in range(PARTS):
            z_copy(z, target, part).start()
        return carry

    lax.fori_loop(z + 1, jnp.minimum(z + 2, outer), z_send, 0)
    if inner == 2:

        @pl.when(y == 0)
        def _():
            wait_ready(me + 1)
            for part in range(PARTS):
                y_copy(z, 0, part).start()

    steps = [rows32[pl.ds(j, runs, stride=SPAN), :] for j in range(SPAN)]
    low8 = low_half((runs, LANES))
    flat_k = jnp.concatenate(
        [
            jnp.where(low8, steps[j], pltpu.roll(steps[j + 1], HEAD_DIM, 1))
            for j in range(0, SPAN, 2)
        ],
        axis=1,
    ).astype(BF16)
    flat_v = jnp.concatenate(
        [
            jnp.where(low8, pltpu.roll(steps[j], HEAD_DIM, 1), steps[j + 1])
            for j in range(0, SPAN, 2)
        ],
        axis=1,
    ).astype(BF16)
    kin_c.wait()
    vin_c.wait()
    kout_c.wait()
    vout_c.wait()
    hidden_k = jax.nn.gelu(dot_t(flat_k, kin[...])).astype(BF16)
    hidden_v = jax.nn.gelu(dot_t(flat_v, vin[...])).astype(BF16)
    sum_k = dot(hidden_k, kout[...]).astype(BF16).astype(F32)
    sum_v = dot(hidden_v, vout[...]).astype(BF16).astype(F32)

    def sum_slot(index):
        return sums.at[pl.ds(pl.multiple_of(index * runs, runs), runs), :]

    sums[pl.ds(pl.multiple_of(me * runs, runs), runs), :] = jnp.concatenate([sum_k, sum_v], axis=1)

    def sum_copy(source, target):
        return pltpu.make_async_remote_copy(
            src_ref=sum_slot(source),
            dst_ref=sum_slot(source),
            send_sem=send_s.at[target],
            recv_sem=recv_s.at[source],
            device_id={"kv": target},
            device_id_type=MESH,
        )

    lax.fori_loop(jnp.minimum(z + 2, outer), jnp.minimum(z + 3, outer), z_send, 0)

    qw_c.wait()
    queries = dot(tok[...], qw[...]) * (HEAD_DIM**-0.5 * LOG2E)
    lax.fori_loop(jnp.minimum(z + 3, outer), outer, z_send, 0)

    def sum_send(target, carry):
        other = lax.rem(target, inner) != y

        @pl.when(other & ((target != me + 1) | (y != 0)))
        def _():
            wait_ready(target)

        sum_copy(me, target).start()
        return carry

    lax.fori_loop(me + 1, n_kv, sum_send, 0)

    low64 = low_half((HEAD_DIM, LANES))
    for b in range(0, blocks, 2):
        for p in range(pairs):
            lanes = slice(p * LANES, (p + 1) * LANES)
            turned = queries[b * BLOCK : (b + 2) * BLOCK, lanes].T
            even, odd = turned[:HEAD_DIM], turned[HEAD_DIM:]
            stacked[b, :HEAD_DIM, lanes] = jnp.where(
                low64, even, pltpu.roll(odd, BLOCK, 1)
            ).astype(BF16)
            stacked[b + 1, :HEAD_DIM, lanes] = jnp.where(
                low64, pltpu.roll(even, BLOCK, 1), odd
            ).astype(BF16)
        stacked[b, HEAD_DIM:, :] = jnp.zeros((HEAD_DIM, cols), BF16)
        stacked[b + 1, HEAD_DIM:, :] = jnp.zeros((HEAD_DIM, cols), BF16)
    gw_c.wait()
    gates = jax.nn.sigmoid(dot_t(gw[...], tok[...]))
    half = gates.shape[0] // 2
    low1 = low_half((1, LANES))
    for branch in range(2):
        at = branch * half
        mine = jnp.where(g == 0, gates[at : at + heads], gates[at + heads : at + 2 * heads])
        for b in range(blocks):
            here = mine[:, b // 2 * LANES : (b // 2 + 1) * LANES]
            moved = pltpu.roll(here, BLOCK, 1)
            left, right = (here, moved) if b % 2 == 0 else (moved, here)
            gate_rows[pl.ds(branch * blocks + b, 1), :] = jnp.concatenate(
                [
                    jnp.where(low1, left[2 * p : 2 * p + 1], right[2 * p + 1 : 2 * p + 2])
                    for p in range(pairs)
                ],
                axis=1,
            )

    def forward(step, carry):
        is_first = jnp.int32(step == 1)
        source = is_first * (z - 1) + (1 - is_first) * (step - 2)
        for part in range(PARTS):
            z_copy(source, z, part).wait_recv()
            if inner == 2:
                y_copy(source, y, part).start()
        return carry

    lax.fori_loop(1, z + 1, forward, 0)

    def sum_wait(source, carry):
        sum_copy(source, me).wait_recv()
        return carry

    lax.fori_loop(0, me, sum_wait, 0)
    sums_kv = sums[...].astype(BF16)
    total_runs = sums_kv.shape[0]
    low_runs = low_half((total_runs, LANES))
    sums_1v = jnp.where(low_runs, jnp.ones_like(sums_kv), sums_kv)
    row_in = lax.rem(lax.broadcasted_iota(jnp.int32, (1, cols), 1), BLOCK)
    run_end = lax.broadcasted_iota(jnp.int32, (total_runs, 1), 0) * SPAN + SPAN - 1
    for b in range(blocks):
        allowed = run_end <= me * local + b * BLOCK + row_in
        shifted = jnp.where(allowed, dot(sums_kv, stacked[b]), -1e30)
        top = jnp.max(shifted, axis=0, keepdims=True)
        weights = jnp.where(allowed, jnp.exp2(shifted - top), 0.0).astype(BF16)
        o_s = dot_rows(sums_1v, weights)
        scale = gate_rows[pl.ds(b, 1), :] / jnp.maximum(o_s[:1], 1.0)
        summary_mix[b] = o_s[HEAD_DIM:] * scale

    sel_c.wait()
    ow_c.wait()
    if inner == 2:

        def y_wait(step, carry):
            for part in range(PARTS):
                y_copy(z - step, 1 - y, part).wait_recv()
            return carry

        lax.fori_loop(1 - y, z + 1, y_wait, 0)

    key_in = lax.broadcasted_iota(jnp.int32, (BLOCK, 1), 0)
    own_allowed = key_in <= row_in
    low_keys = low_half((picks * BLOCK, LANES))
    mixes = []
    for b in range(blocks):
        rows = slice(b * BLOCK, (b + 1) * BLOCK)
        chosen = [sel[0, b, s] for s in range(picks)]
        kv = jnp.concatenate([gathered[jnp.maximum(c, 0)] for c in chosen], axis=0)
        raw = dot(kv, stacked[b])
        scores = jnp.concatenate(
            [jnp.where(own_allowed, raw[:BLOCK], -1e30)]
            + [
                raw[s * BLOCK : (s + 1) * BLOCK] + jnp.where(chosen[s] >= 0, 0.0, -1e30)
                for s in range(1, picks)
            ],
            axis=0,
        )
        top = jnp.max(scores, axis=0, keepdims=True)
        weights = jnp.exp2(scores - top).astype(BF16)
        o_c = dot_rows(jnp.where(low_keys, jnp.ones_like(kv), kv), weights)
        scale = gate_rows[pl.ds(blocks + b, 1), :] / o_c[:1]
        mixed = summary_mix[b] + o_c[HEAD_DIM:] * scale
        for p in range(0, pairs, 2):
            one = mixed[:, p * LANES : (p + 1) * LANES]
            two = mixed[:, (p + 1) * LANES : (p + 2) * LANES]
            turned = jnp.concatenate(
                [
                    jnp.where(low64, one, pltpu.roll(two, BLOCK, 1)),
                    jnp.where(low64, pltpu.roll(one, BLOCK, 1), two),
                ],
                axis=0,
            ).T.astype(BF16)
            own_mix[rows, p * LANES : (p + 1) * LANES] = turned[:BLOCK]
            own_mix[rows, (p + 1) * LANES : (p + 2) * LANES] = turned[BLOCK:]
        mix = pltpu.make_async_remote_copy(
            src_ref=own_mix.at[rows],
            dst_ref=peer_mix.at[rows],
            send_sem=send_m.at[b],
            recv_sem=recv_m.at[b],
            device_id={"tp": 1 - g},
            device_id_type=MESH,
        )
        mix.start()
        mixes.append(mix)

    own_rows = pl.ds(pl.multiple_of(g * cols, cols), cols)
    peer_rows = pl.ds(pl.multiple_of((1 - g) * cols, cols), cols)
    partial[...] = dot(own_mix[...], ow[own_rows, :])
    for mix in mixes:
        mix.wait_recv()
    out_ref[...] = (partial[...] + dot(peer_mix[...], ow[peer_rows, :])).astype(BF16)
    for mix in mixes:
        mix.wait_send()

    def z_done(target, carry):
        for part in range(PARTS):
            z_copy(z, target, part).wait_send()
        return carry

    lax.fori_loop(z + 1, outer, z_done, 0)

    def sum_done(target, carry):
        sum_copy(me, target).wait_send()
        return carry

    lax.fori_loop(me + 1, n_kv, sum_done, 0)
    if inner == 2:

        def y_done(step, carry):
            for part in range(PARTS):
                y_copy(z - step, y, part).wait_send()
            return carry

        lax.fori_loop(y, z + 1, y_done, 0)


def per_device(n_kv, tokens, qw, kw, vw, gw, kin, kout, vin, vout, ow, selection):
    gw, kin, vin = gw.T, kin.T, vin.T
    local, width = tokens.shape
    cols = qw.shape[1]
    inner = 2 if n_kv % 2 == 0 else 1
    outer = n_kv // inner
    blocks = local // BLOCK
    runs = local // SPAN
    hbm = pl.BlockSpec(memory_space=pltpu.HBM)
    dma = pltpu.SemaphoreType.DMA
    vm = pltpu.VMEM
    operands = [
        pltpu.with_memory_space_constraint(a, pltpu.HBM)
        for a in (selection, tokens, qw, kw, vw, gw, kin, kout, vin, vout, ow)
    ]
    return pl.pallas_call(
        functools.partial(kernel, n_kv, inner),
        out_shape=pltpu.VMEM((local, ow.shape[1]), BF16),
        in_specs=[hbm] * 11,
        out_specs=pl.BlockSpec(memory_space=pltpu.VMEM),
        scratch_shapes=[
            pltpu.SMEM(selection.shape, jnp.int32),
            vm(tokens.shape, BF16),
            vm(qw.shape, BF16),
            vm((width, 2 * LANES), BF16),
            vm(gw.shape, BF16),
            vm(kin.shape, BF16),
            vm(kout.shape, BF16),
            vm(vin.shape, BF16),
            vm(vout.shape, BF16),
            vm(ow.shape, BF16),
            vm((local, LANES), F32),
            vm((n_kv * blocks, BLOCK, LANES), BF16),
            vm((n_kv * runs, LANES), F32),
            vm((blocks, LANES, cols), BF16),
            vm((blocks, HEAD_DIM, cols), F32),
            vm((2 * blocks, cols), F32),
            vm((local, cols), BF16),
            vm((local, cols), BF16),
            vm((local, ow.shape[1]), F32),
            dma((3 * CHUNKS + 8,)),
            pltpu.SemaphoreType.REGULAR((n_kv,)),
            dma((outer, PARTS)),
            dma((outer, PARTS)),
            dma((outer, PARTS)),
            dma((outer, PARTS)),
            dma((n_kv,)),
            dma((n_kv,)),
            dma((blocks,)),
            dma((blocks,)),
        ],
        compiler_params=pltpu.CompilerParams(
            collective_id=0, has_side_effects=True, vmem_limit_bytes=GRANT
        ),
        name="attend",
    )(*operands)


def solution(mesh):
    in_specs = (
        P(("dp", "kv"), None),
        P(None, "tp"),
        P(),
        P(),
        P(),
        P(),
        P(),
        P(),
        P(),
        P(None, "tp"),
        P("tp", ("dp", "kv"), None),
    )
    out_specs = P(("dp", "kv"), "tp")
    return jax.shard_map(
        functools.partial(per_device, mesh.shape["kv"]),
        mesh=mesh,
        in_specs=in_specs,
        out_specs=out_specs,
        check_vma=False,
    )
```

time: 22.9 us -> 19.5 us (0.85)
  Pallas kernels: 20.8 us -> 18.6 us
  local copies, waits for them, and re-layouts: 1.87 us -> 0.8 us
    pallas_call x1, Pallas kernels: 20.8 us -> 18.6 us  [per_device(): pl.pallas_call(functools.partial(kernel, n_kv, inner), out_shape=pltpu.VM...]
    unnamed x1, local copies, waits for them, and re-layouts: 1.87 us -> 0.8 us
where the time goes in v1:
time: 19.5 us; the launch traced here: 19.4 us
  Pallas kernels  18.6 us (95%)
  local copies, waits for them, and re-layouts  0.8 us (4%)
    pallas_call x1, Pallas kernels, per_device(): pl.pallas_call(functools.partial(kernel, n_kv, inner), out_shape=pltpu.VM...  18.6 us
    unnamed x1, local copies, waits for them, and re-layouts  0.8 us

profile of v1, /device:TPU:25, one launch (start us, length us, event | category | flops | bytes accessed | tf_op | source)
XLA Modules:
  0.0 19.4 jit_solution(15200981254824138778)
XLA Ops:
  0.0 18.6 %attend.1 = bf16[256,1024]{1,0:T(8,128)(2,1)S(1)} custom-call(s32[1,4,8]{2,1,0:T(4,128)} %sel_hbm.1, bf16[256,2048]{1,0:T(8,128)(2,1)} %tok_hbm.1, bf16[2048,512]{1,0:T(8,128)(2,1)} %qw_hbm.1, bf16[2048,128]{1,0:T(8,128)(2,1)} %kw_hbm.1, bf16[2048,128]{1,0:T(8,128)(2,1)} %vw_hbm.1, bf16[32,2048]{1,0:T(8,128)(2,1)} %bitcast.5, bf16[64,2048]{1,0:T(8,128)(2,1)} %bitcast.3, ...), custom_call_target="tpu_custom_call" | custom-call | tf_op jit(solution)/shard_map/attend/pallas_call | solution.py:436
  18.6 0.8 %copy.13 = bf16[256,1024]{1,0:T(8,128)(2,1)} copy(bf16[256,1024]{1,0:T(8,128)(2,1)S(1)} %attend.1) | data formatting | bytes 1048576

commit v2 on v1

--- a/solution.py
+++ b/solution.py
@@ -16,6 +16,7 @@
 BF16 = jnp.bfloat16
 CHUNKS = 4
 PARTS = 2
+AHEAD = 8
 LOG2E = 1.4426950408889634
 GRANT = 40 * 1024 * 1024
 
@@ -26,10 +27,6 @@
 
 def dot_t(a, b):
     return lax.dot_general(a, b, (((1,), (1,)), ((), ())), preferred_element_type=F32)
-
-
-def dot_rows(a, b):
-    return lax.dot_general(a, b, (((0,), (0,)), ((), ())), preferred_element_type=F32)
 
 
 def low_half(shape):
@@ -66,7 +63,7 @@
     sums,
     stacked,
     summary_mix,
-    gate_rows,
+    gate_wide,
     own_mix,
     peer_mix,
     partial,
@@ -267,38 +264,30 @@
 
     lax.fori_loop(me + 1, n_kv, sum_send, 0)
 
-    low64 = low_half((HEAD_DIM, LANES))
-    for b in range(0, blocks, 2):
+    low64 = low_half((BLOCK, LANES))
+    row_in = lax.broadcasted_iota(jnp.int32, (BLOCK, 1), 0)
+    lane = lax.broadcasted_iota(jnp.int32, (1, LANES), 1)
+    unit = jnp.where(lane - HEAD_DIM == row_in, 1.0, 0.0)
+    for b in range(blocks):
+        rows = slice(b * BLOCK, (b + 1) * BLOCK)
         for p in range(pairs):
-            lanes = slice(p * LANES, (p + 1) * LANES)
-            turned = queries[b * BLOCK : (b + 2) * BLOCK, lanes].T
-            even, odd = turned[:HEAD_DIM], turned[HEAD_DIM:]
-            stacked[b, :HEAD_DIM, lanes] = jnp.where(
-                low64, even, pltpu.roll(odd, BLOCK, 1)
+            two = queries[rows, p * LANES : (p + 1) * LANES]
+            at = 2 * p * BLOCK
+            stacked[b, at : at + BLOCK] = jnp.where(low64, two, unit).astype(BF16)
+            stacked[b, at + BLOCK : at + 2 * BLOCK] = jnp.where(
+                low64, pltpu.roll(two, HEAD_DIM, 1), unit
             ).astype(BF16)
-            stacked[b + 1, :HEAD_DIM, lanes] = jnp.where(
-                low64, pltpu.roll(even, BLOCK, 1), odd
-            ).astype(BF16)
-        stacked[b, HEAD_DIM:, :] = jnp.zeros((HEAD_DIM, cols), BF16)
-        stacked[b + 1, HEAD_DIM:, :] = jnp.zeros((HEAD_DIM, cols), BF16)
     gw_c.wait()
-    gates = jax.nn.sigmoid(dot_t(gw[...], tok[...]))
-    half = gates.shape[0] // 2
-    low1 = low_half((1, LANES))
-    for branch in range(2):
-        at = branch * half
-        mine = jnp.where(g == 0, gates[at : at + heads], gates[at + heads : at + 2 * heads])
-        for b in range(blocks):
-            here = mine[:, b // 2 * LANES : (b // 2 + 1) * LANES]
-            moved = pltpu.roll(here, BLOCK, 1)
-            left, right = (here, moved) if b % 2 == 0 else (moved, here)
-            gate_rows[pl.ds(branch * blocks + b, 1), :] = jnp.concatenate(
-                [
-                    jnp.where(low1, left[2 * p : 2 * p + 1], right[2 * p + 1 : 2 * p + 2])
-                    for p in range(pairs)
-                ],
-                axis=1,
-            )
+    gates = jax.nn.sigmoid(dot_t(tok[...], gw[...]))
+    half = gates.shape[1] // 2
+    gate_s = jnp.where(g == 0, gates[:, :heads], gates[:, heads:half])
+    gate_c = jnp.where(g == 0, gates[:, half : half + heads], gates[:, half + heads :])
+    for b in range(blocks):
+        rows = slice(b * BLOCK, (b + 1) * BLOCK)
+        for h in range(heads):
+            at = slice(h * BLOCK, (h + 1) * BLOCK)
+            gate_wide[b, at] = jnp.broadcast_to(gate_c[rows, h : h + 1], (BLOCK, LANES))
+            summary_mix[b, at] = jnp.broadcast_to(gate_s[rows, h : h + 1], (BLOCK, LANES))
 
     def forward(step, carry):
         is_first = jnp.int32(step == 1)
@@ -319,17 +308,18 @@
     sums_kv = sums[...].astype(BF16)
     total_runs = sums_kv.shape[0]
     low_runs = low_half((total_runs, LANES))
-    sums_1v = jnp.where(low_runs, jnp.ones_like(sums_kv), sums_kv)
-    row_in = lax.rem(lax.broadcasted_iota(jnp.int32, (1, cols), 1), BLOCK)
+    sums_1 = jnp.concatenate([sums_kv, jnp.ones_like(sums_kv)], axis=1)
     run_end = lax.broadcasted_iota(jnp.int32, (total_runs, 1), 0) * SPAN + SPAN - 1
+    tall_row = lax.rem(lax.broadcasted_iota(jnp.int32, (heads * BLOCK, 1), 0), BLOCK)
     for b in range(blocks):
-        allowed = run_end <= me * local + b * BLOCK + row_in
-        shifted = jnp.where(allowed, dot(sums_kv, stacked[b]), -1e30)
-        top = jnp.max(shifted, axis=0, keepdims=True)
-        weights = jnp.where(allowed, jnp.exp2(shifted - top), 0.0).astype(BF16)
-        o_s = dot_rows(sums_1v, weights)
-        scale = gate_rows[pl.ds(b, 1), :] / jnp.maximum(o_s[:1], 1.0)
-        summary_mix[b] = o_s[HEAD_DIM:] * scale
+        first_row = me * local + b * BLOCK
+        barred = jnp.where(run_end <= first_row + lane - HEAD_DIM, 0.0, -1e30).astype(BF16)
+        scores = dot_t(stacked[b], jnp.where(low_runs, sums_kv, barred))
+        top = jnp.max(scores, axis=1, keepdims=True)
+        weights = jnp.exp2(scores - top).astype(BF16)
+        o_s = dot(weights, sums_1)
+        part = summary_mix[b] * o_s[:, :LANES] / o_s[:, LANES:]
+        summary_mix[b] = jnp.where(first_row + tall_row >= SPAN - 1, part, 0.0)
 
     sel_c.wait()
     ow_c.wait()
@@ -342,40 +332,49 @@
 
         lax.fori_loop(1 - y, z + 1, y_wait, 0)
 
-    key_in = lax.broadcasted_iota(jnp.int32, (BLOCK, 1), 0)
-    own_allowed = key_in <= row_in
-    low_keys = low_half((picks * BLOCK, LANES))
+    later_key = jnp.where(row_in <= lane - HEAD_DIM, 0.0, -1e30).astype(BF16)
+    tall = 2 * LANES
+    pieces = [(b, c) for b in range(blocks) for c in range(cols // tall)]
+    left, right = {}, {}
+
+    def scores_of(b, c):
+        if c == 0:
+            score_rows, value_rows = [], []
+            for s in range(picks):
+                index = sel[0, b, s]
+                kv = gathered[jnp.maximum(index, 0)]
+                bar = later_key
+                if s > 0:
+                    bar = jnp.full((BLOCK, LANES), jnp.where(index >= 0, 0.0, -1e30), F32)
+                    bar = bar.astype(BF16)
+                score_rows.append(jnp.where(low64, kv, bar))
+                value_rows.append(kv)
+            left[b] = jnp.concatenate(score_rows, axis=0)
+            kv = jnp.concatenate(value_rows, axis=0)
+            right[b] = jnp.concatenate([kv, jnp.ones_like(kv)], axis=1)
+        return dot_t(stacked[b, c * tall : (c + 1) * tall, :], left[b])
+
     mixes = []
-    for b in range(blocks):
+    queue = [scores_of(*piece) for piece in pieces[:AHEAD]]
+    for i, (b, c) in enumerate(pieces):
         rows = slice(b * BLOCK, (b + 1) * BLOCK)
-        chosen = [sel[0, b, s] for s in range(picks)]
-        kv = jnp.concatenate([gathered[jnp.maximum(c, 0)] for c in chosen], axis=0)
-        raw = dot(kv, stacked[b])
-        scores = jnp.concatenate(
-            [jnp.where(own_allowed, raw[:BLOCK], -1e30)]
-            + [
-                raw[s * BLOCK : (s + 1) * BLOCK] + jnp.where(chosen[s] >= 0, 0.0, -1e30)
-                for s in range(1, picks)
-            ],
-            axis=0,
-        )
-        top = jnp.max(scores, axis=0, keepdims=True)
+        at = slice(c * tall, (c + 1) * tall)
+        scores = queue.pop(0)
+        if i + AHEAD < len(pieces):
+            queue.append(scores_of(*pieces[i + AHEAD]))
+        top = jnp.max(scores, axis=1, keepdims=True)
         weights = jnp.exp2(scores - top).astype(BF16)
-        o_c = dot_rows(jnp.where(low_keys, jnp.ones_like(kv), kv), weights)
-        scale = gate_rows[pl.ds(blocks + b, 1), :] / o_c[:1]
-        mixed = summary_mix[b] + o_c[HEAD_DIM:] * scale
-        for p in range(0, pairs, 2):
-            one = mixed[:, p * LANES : (p + 1) * LANES]
-            two = mixed[:, (p + 1) * LANES : (p + 2) * LANES]
-            turned = jnp.concatenate(
-                [
-                    jnp.where(low64, one, pltpu.roll(two, BLOCK, 1)),
-                    jnp.where(low64, pltpu.roll(one, BLOCK, 1), two),
-                ],
-                axis=0,
-            ).T.astype(BF16)
-            own_mix[rows, p * LANES : (p + 1) * LANES] = turned[:BLOCK]
-            own_mix[rows, (p + 1) * LANES : (p + 2) * LANES] = turned[BLOCK:]
+        o_c = dot(weights, right[b])
+        mixed = summary_mix[b, at] + gate_wide[b, at] * (o_c[:, :LANES] / o_c[:, LANES:])
+        for p in range(tall // LANES):
+            even = mixed[2 * p * BLOCK : (2 * p + 1) * BLOCK]
+            odd_head = mixed[(2 * p + 1) * BLOCK : (2 * p + 2) * BLOCK]
+            here = (c * tall // LANES + p) * LANES
+            own_mix[rows, here : here + LANES] = jnp.where(
+                low64, pltpu.roll(even, HEAD_DIM, 1), odd_head
+            ).astype(BF16)
+        if c < cols // tall - 1:
+            continue
         mix = pltpu.make_async_remote_copy(
             src_ref=own_mix.at[rows],
             dst_ref=peer_mix.at[rows],
@@ -426,6 +425,7 @@
     outer = n_kv // inner
     blocks = local // BLOCK
     runs = local // SPAN
+    tall = cols // HEAD_DIM * BLOCK
     hbm = pl.BlockSpec(memory_space=pltpu.HBM)
     dma = pltpu.SemaphoreType.DMA
     vm = pltpu.VMEM
@@ -452,9 +452,9 @@
             vm((local, LANES), F32),
             vm((n_kv * blocks, BLOCK, LANES), BF16),
             vm((n_kv * runs, LANES), F32),
-            vm((blocks, LANES, cols), BF16),
-            vm((blocks, HEAD_DIM, cols), F32),
-            vm((2 * blocks, cols), F32),
+            vm((blocks, tall, LANES), BF16),
+            vm((blocks, tall, LANES), F32),
+            vm((blocks, tall, LANES), F32),
             vm((local, cols), BF16),
             vm((local, cols), BF16),
             vm((local, ow.shape[1]), F32),

time: 19.5 us -> 18 us (0.923)
  Pallas kernels: 18.6 us -> 17.1 us
    pallas_call x1, Pallas kernels: 18.6 us -> 17.1 us  [per_device(): pl.pallas_call(functools.partial(kernel, n_kv, inner), out_shape=pltpu.VM...]
where the time goes in v2:
time: 18 us; the launch traced here: 17.9 us
  Pallas kernels  17.1 us (95%)
  local copies, waits for them, and re-layouts  0.8 us (4%)
    pallas_call x1, Pallas kernels, per_device(): pl.pallas_call(functools.partial(kernel, n_kv, inner), out_shape=pltpu.VM...  17.1 us
    unnamed x1, local copies, waits for them, and re-layouts  0.8 us

profile of v2, /device:TPU:25, one launch (start us, length us, event | category | flops | bytes accessed | tf_op | source)
XLA Modules:
  0.0 17.9 jit_solution(1676540528871918118)
XLA Ops:
  0.0 17.1 %attend.1 = bf16[256,1024]{1,0:T(8,128)(2,1)S(1)} custom-call(s32[1,4,8]{2,1,0:T(4,128)} %sel_hbm.1, bf16[256,2048]{1,0:T(8,128)(2,1)} %tok_hbm.1, bf16[2048,512]{1,0:T(8,128)(2,1)} %qw_hbm.1, bf16[2048,128]{1,0:T(8,128)(2,1)} %kw_hbm.1, bf16[2048,128]{1,0:T(8,128)(2,1)} %vw_hbm.1, bf16[32,2048]{1,0:T(8,128)(2,1)} %bitcast.5, bf16[64,2048]{1,0:T(8,128)(2,1)} %bitcast.3, ...), custom_call_target="tpu_custom_call" | custom-call | tf_op jit(solution)/shard_map/attend/pallas_call | solution.py:436
  17.1 0.8 %copy.13 = bf16[256,1024]{1,0:T(8,128)(2,1)} copy(bf16[256,1024]{1,0:T(8,128)(2,1)S(1)} %attend.1) | data formatting | bytes 1048576

commit v3 on v2

--- a/solution.py
+++ b/solution.py
@@ -15,7 +15,8 @@
 F32 = jnp.float32
 BF16 = jnp.bfloat16
 CHUNKS = 4
-PARTS = 2
+PARTS = 4
+SEND_ORDER = ((0, 0, 1), (0, 0, 4))
 AHEAD = 8
 LOG2E = 1.4426950408889634
 GRANT = 40 * 1024 * 1024
@@ -91,13 +92,25 @@
     z = me // inner
     y = lax.rem(me, inner)
 
+    sums[...] = jnp.zeros_like(sums)
     barrier = pltpu.get_barrier_semaphore()
 
     def greet(target, carry):
-        pl.semaphore_signal(barrier, inc=1, device_id={"kv": target}, device_id_type=MESH)
-        return carry
-
-    lax.fori_loop(me + 1, n_kv, greet, 0)
+        pl.semaphore_signal(
+            barrier, inc=1, device_id={"kv": target * inner + y}, device_id_type=MESH
+        )
+        return carry
+
+    def partner():
+        return {"kv": z * inner + lax.rem(y + 1, inner)}
+
+    lax.fori_loop(z + 1, outer, greet, 0)
+    if inner == 2:
+
+        @pl.when(y == 0)
+        def _():
+            pl.semaphore_signal(barrier, inc=1, device_id=partner(), device_id_type=MESH)
+
     pl.semaphore_signal(barrier, inc=1, device_id={"tp": 1 - g}, device_id_type=MESH)
 
     depth = width // CHUNKS
@@ -105,18 +118,20 @@
     for c in range(CHUNKS):
         part = pl.ds(c * depth, depth)
         trio = [
-            pltpu.make_async_copy(tok_hbm.at[:, part], tok.at[:, part], load_sem.at[3 * c]),
+            pltpu.make_async_copy(tok_hbm.at[:, part], tok.at[:, part], load_sem.at[c]),
             pltpu.make_async_copy(
-                kw_hbm.at[part], kvw.at[part, pl.ds(0, LANES)], load_sem.at[3 * c + 1]
+                kw_hbm.at[part], kvw.at[part, pl.ds(0, LANES)], load_sem.at[c]
             ),
             pltpu.make_async_copy(
-                vw_hbm.at[part], kvw.at[part, pl.ds(LANES, LANES)], load_sem.at[3 * c + 2]
+                vw_hbm.at[part], kvw.at[part, pl.ds(LANES, LANES)], load_sem.at[c]
             ),
         ]
         for copy in trio:
             copy.start()
         first.append(trio)
-    base = 3 * CHUNKS
+    base = CHUNKS
+    span_rows = depth * (local + 2 * LANES) // (2 * LANES)
+    whole_chunk = kvw.at[pl.ds(0, span_rows)]
     later = [
         pltpu.make_async_copy(src, dst, load_sem.at[base + i])
         for i, (src, dst) in enumerate(
@@ -134,21 +149,30 @@
     ]
     kin_c, vin_c, kout_c, vout_c, qw_c, gw_c, sel_c, ow_c = later
 
-    sums[...] = jnp.zeros_like(sums)
-    pl.semaphore_wait(barrier, me + 1)
-
-    def tell(target, carry):
-        pl.semaphore_signal(ready.at[me], inc=1, device_id={"kv": target}, device_id_type=MESH)
-        return carry
-
-    lax.fori_loop(0, me, tell, 0)
+
+    pl.semaphore_wait(barrier, z + y + 1)
+
+    def tell(step, carry):
+        pl.semaphore_signal(
+            ready.at[z], inc=1, device_id={"kv": (z - step) * inner + y}, device_id_type=MESH
+        )
+        return carry
+
+    lax.fori_loop(1, z + 1, tell, 0)
+    if inner == 2:
+
+        @pl.when(y == 1)
+        def _():
+            pl.semaphore_signal(ready.at[z], inc=1, device_id=partner(), device_id_type=MESH)
 
     acc = jnp.zeros((local, 2 * LANES), F32)
     for c in range(CHUNKS):
-        for copy in first[c]:
-            copy.wait()
+        pltpu.make_async_copy(whole_chunk, whole_chunk, load_sem.at[c]).wait()
+        if c == 0:
+            for copy in later[:4]:
+                copy.start()
         if c == CHUNKS - 2:
-            for copy in later:
+            for copy in later[4:]:
                 copy.start()
         part = pl.ds(c * depth, depth)
         acc += dot(tok[:, part], kvw[part, :])
@@ -165,6 +189,9 @@
 
     part_blocks = blocks // PARTS
 
+    def full(index):
+        return gathered.at[pl.ds(index * blocks, blocks)]
+
     def slot(index, part):
         return gathered.at[pl.ds(index * blocks + part * part_blocks, part_blocks)]
 
@@ -172,7 +199,7 @@
         return pltpu.make_async_remote_copy(
             src_ref=slot(source_z * inner + y, part),
             dst_ref=slot(source_z * inner + y, part),
-            send_sem=send_z.at[target_z, part],
+            send_sem=send_z.at[target_z],
             recv_sem=recv_z.at[source_z, part],
             device_id={"kv": target_z * inner + y},
             device_id_type=MESH,
@@ -182,30 +209,44 @@
         return pltpu.make_async_remote_copy(
             src_ref=slot(source_z * inner + source_y, part),
             dst_ref=slot(source_z * inner + source_y, part),
-            send_sem=send_y.at[source_z, part],
-            recv_sem=recv_y.at[source_z, part],
+            send_sem=send_y.at[source_z],
+            recv_sem=recv_y.at[source_z],
             device_id={"kv": z * inner + lax.rem(y + 1, inner)},
             device_id_type=MESH,
         )
 
-    def wait_ready(index):
-        pl.semaphore_wait(ready.at[index], 1)
-
     def z_send(target, carry):
-        wait_ready(target * inner + y)
+        pl.semaphore_wait(ready.at[target], 1)
         for part in range(PARTS):
             z_copy(z, target, part).start()
         return carry
 
-    lax.fori_loop(z + 1, jnp.minimum(z + 2, outer), z_send, 0)
-    if inner == 2:
-
-        @pl.when(y == 0)
-        def _():
-            wait_ready(me + 1)
-            for part in range(PARTS):
-                y_copy(z, 0, part).start()
-
+    def send_near():
+        lax.fori_loop(jnp.minimum(z + 1, outer), jnp.minimum(z + 2, outer), z_send, 0)
+
+    def send_far():
+        lax.fori_loop(jnp.minimum(z + 2, outer), outer, z_send, 0)
+
+    def send_across():
+        if inner == 2:
+
+            @pl.when(y == 0)
+            def _():
+                pl.semaphore_wait(ready.at[z], 1)
+                for part in range(PARTS):
+                    y_copy(z, 0, part).start()
+
+    def send_at(point):
+        for core, order in enumerate(SEND_ORDER):
+            jobs = [job for at, job in zip(order, (send_near, send_across, send_far)) if at == point]
+            if jobs:
+
+                @pl.when(g == core)
+                def _():
+                    for job in jobs:
+                        job()
+
+    send_at(0)
     steps = [rows32[pl.ds(j, runs, stride=SPAN), :] for j in range(SPAN)]
     low8 = low_half((runs, LANES))
     flat_k = jnp.concatenate(
@@ -231,39 +272,41 @@
     sum_k = dot(hidden_k, kout[...]).astype(BF16).astype(F32)
     sum_v = dot(hidden_v, vout[...]).astype(BF16).astype(F32)
 
-    def sum_slot(index):
-        return sums.at[pl.ds(pl.multiple_of(index * runs, runs), runs), :]
-
-    sums[pl.ds(pl.multiple_of(me * runs, runs), runs), :] = jnp.concatenate([sum_k, sum_v], axis=1)
+    mine = pl.ds(pl.multiple_of(me * runs, runs), runs)
+    sums[mine, :] = jnp.concatenate([sum_k, sum_v], axis=1)
+    yours = pl.ds(pl.multiple_of((z * inner + lax.rem(y + 1, inner)) * runs, runs), runs)
+
+    def sum_swap(slot):
+        return pltpu.make_async_remote_copy(
+            src_ref=sums.at[slot, :],
+            dst_ref=sums.at[slot, :],
+            send_sem=send_s.at[z],
+            recv_sem=recv_s.at[z],
+            device_id=partner(),
+            device_id_type=MESH,
+        )
+
+    if inner == 2:
+        sum_swap(mine).start()
 
     def sum_copy(source, target):
+        both = inner * runs
+        slot = sums.at[pl.ds(pl.multiple_of(source * both, both), both), :]
         return pltpu.make_async_remote_copy(
-            src_ref=sum_slot(source),
-            dst_ref=sum_slot(source),
+            src_ref=slot,
+            dst_ref=slot,
             send_sem=send_s.at[target],
             recv_sem=recv_s.at[source],
-            device_id={"kv": target},
+            device_id={"kv": target * inner + y},
             device_id_type=MESH,
         )
 
-    lax.fori_loop(jnp.minimum(z + 2, outer), jnp.minimum(z + 3, outer), z_send, 0)
+    send_at(1)
 
     qw_c.wait()
     queries = dot(tok[...], qw[...]) * (HEAD_DIM**-0.5 * LOG2E)
-    lax.fori_loop(jnp.minimum(z + 3, outer), outer, z_send, 0)
-
-    def sum_send(target, carry):
-        other = lax.rem(target, inner) != y
-
-        @pl.when(other & ((target != me + 1) | (y != 0)))
-        def _():
-            wait_ready(target)
-
-        sum_copy(me, target).start()
-        return carry
-
-    lax.fori_loop(me + 1, n_kv, sum_send, 0)
-
+
+    send_at(2)
     low64 = low_half((BLOCK, LANES))
     row_in = lax.broadcasted_iota(jnp.int32, (BLOCK, 1), 0)
     lane = lax.broadcasted_iota(jnp.int32, (1, LANES), 1)
@@ -277,6 +320,7 @@
             stacked[b, at + BLOCK : at + 2 * BLOCK] = jnp.where(
                 low64, pltpu.roll(two, HEAD_DIM, 1), unit
             ).astype(BF16)
+    send_at(3)
     gw_c.wait()
     gates = jax.nn.sigmoid(dot_t(tok[...], gw[...]))
     half = gates.shape[1] // 2
@@ -289,6 +333,15 @@
             gate_wide[b, at] = jnp.broadcast_to(gate_c[rows, h : h + 1], (BLOCK, LANES))
             summary_mix[b, at] = jnp.broadcast_to(gate_s[rows, h : h + 1], (BLOCK, LANES))
 
+    def sum_send(target, carry):
+        sum_copy(z, target).start()
+        return carry
+
+    send_at(4)
+    if inner == 2:
+        sum_swap(yours).wait_recv()
+    lax.fori_loop(z + 1, outer, sum_send, 0)
+
     def forward(step, carry):
         is_first = jnp.int32(step == 1)
         source = is_first * (z - 1) + (1 - is_first) * (step - 2)
@@ -301,10 +354,10 @@
     lax.fori_loop(1, z + 1, forward, 0)
 
     def sum_wait(source, carry):
-        sum_copy(source, me).wait_recv()
-        return carry
-
-    lax.fori_loop(0, me, sum_wait, 0)
+        sum_copy(source, z).wait_recv()
+        return carry
+
+    lax.fori_loop(0, z, sum_wait, 0)
     sums_kv = sums[...].astype(BF16)
     total_runs = sums_kv.shape[0]
     low_runs = low_half((total_runs, LANES))
@@ -326,8 +379,7 @@
     if inner == 2:
 
         def y_wait(step, carry):
-            for part in range(PARTS):
-                y_copy(z - step, 1 - y, part).wait_recv()
+            pltpu.make_async_copy(full(me), full(me), recv_y.at[z - step]).wait()
             return carry
 
         lax.fori_loop(1 - y, z + 1, y_wait, 0)
@@ -354,7 +406,6 @@
             right[b] = jnp.concatenate([kv, jnp.ones_like(kv)], axis=1)
         return dot_t(stacked[b, c * tall : (c + 1) * tall, :], left[b])
 
-    mixes = []
     queue = [scores_of(*piece) for piece in pieces[:AHEAD]]
     for i, (b, c) in enumerate(pieces):
         rows = slice(b * BLOCK, (b + 1) * BLOCK)
@@ -378,40 +429,44 @@
         mix = pltpu.make_async_remote_copy(
             src_ref=own_mix.at[rows],
             dst_ref=peer_mix.at[rows],
-            send_sem=send_m.at[b],
-            recv_sem=recv_m.at[b],
+            send_sem=send_m.at[0],
+            recv_sem=recv_m.at[0],
             device_id={"tp": 1 - g},
             device_id_type=MESH,
         )
         mix.start()
-        mixes.append(mix)
 
     own_rows = pl.ds(pl.multiple_of(g * cols, cols), cols)
     peer_rows = pl.ds(pl.multiple_of((1 - g) * cols, cols), cols)
     partial[...] = dot(own_mix[...], ow[own_rows, :])
-    for mix in mixes:
-        mix.wait_recv()
+    all_mixes = pltpu.make_async_remote_copy(
+        src_ref=own_mix,
+        dst_ref=peer_mix,
+        send_sem=send_m.at[0],
+        recv_sem=recv_m.at[0],
+        device_id={"tp": 1 - g},
+        device_id_type=MESH,
+    )
+    all_mixes.wait_recv()
     out_ref[...] = (partial[...] + dot(peer_mix[...], ow[peer_rows, :])).astype(BF16)
-    for mix in mixes:
-        mix.wait_send()
+    all_mixes.wait_send()
 
     def z_done(target, carry):
-        for part in range(PARTS):
-            z_copy(z, target, part).wait_send()
+        pltpu.make_async_copy(full(me), full(me), send_z.at[target]).wait()
         return carry
 
     lax.fori_loop(z + 1, outer, z_done, 0)
 
     def sum_done(target, carry):
-        sum_copy(me, target).wait_send()
-        return carry
-
-    lax.fori_loop(me + 1, n_kv, sum_done, 0)
+        sum_copy(z, target).wait_send()
+        return carry
+
+    lax.fori_loop(z + 1, outer, sum_done, 0)
     if inner == 2:
+        sum_swap(mine).wait_send()
 
         def y_done(step, carry):
-            for part in range(PARTS):
-                y_copy(z - step, y, part).wait_send()
+            pltpu.make_async_copy(full(me), full(me), send_y.at[z - step]).wait()
             return carry
 
         lax.fori_loop(y, z + 1, y_done, 0)
@@ -458,16 +513,16 @@
             vm((local, cols), BF16),
             vm((local, cols), BF16),
             vm((local, ow.shape[1]), F32),
-            dma((3 * CHUNKS + 8,)),
-            pltpu.SemaphoreType.REGULAR((n_kv,)),
+            dma((CHUNKS + 8,)),
+            pltpu.SemaphoreType.REGULAR((outer,)),
+            dma((outer,)),
             dma((outer, PARTS)),
-            dma((outer, PARTS)),
-            dma((outer, PARTS)),
-            dma((outer, PARTS)),
-            dma((n_kv,)),
-            dma((n_kv,)),
-            dma((blocks,)),
-            dma((blocks,)),
+            dma((outer,)),
+            dma((outer,)),
+            dma((outer,)),
+            dma((outer,)),
+            dma((1,)),
+            dma((1,)),
         ],
         compiler_params=pltpu.CompilerParams(
             collective_id=0, has_side_effects=True, vmem_limit_bytes=GRANT

time: 18 us -> 17.4 us (0.967)
  Pallas kernels: 17.1 us -> 16.5 us
    pallas_call x1, Pallas kernels: 17.1 us -> 16.5 us  [per_device(): pl.pallas_call(functools.partial(kernel, n_kv, inner), out_shape=pltpu.VM...]
where the time goes in v3:
time: 17.4 us; the launch traced here: 17.3 us
  Pallas kernels  16.5 us (95%)
  local copies, waits for them, and re-layouts  0.8 us (5%)
    pallas_call x1, Pallas kernels, per_device(): pl.pallas_call(functools.partial(kernel, n_kv, inner), out_shape=pltpu.VM...  16.5 us
    unnamed x1, local copies, waits for them, and re-layouts  0.8 us

profile of v3, /device:TPU:25, one launch (start us, length us, event | category | flops | bytes accessed | tf_op | source)
XLA Modules:
  0.0 17.3 jit_solution(2998921543391753058)
XLA Ops:
  0.0 16.5 %attend.1 = bf16[256,1024]{1,0:T(8,128)(2,1)S(1)} custom-call(s32[1,4,8]{2,1,0:T(4,128)} %sel_hbm.1, bf16[256,2048]{1,0:T(8,128)(2,1)} %tok_hbm.1, bf16[2048,512]{1,0:T(8,128)(2,1)} %qw_hbm.1, bf16[2048,128]{1,0:T(8,128)(2,1)} %kw_hbm.1, bf16[2048,128]{1,0:T(8,128)(2,1)} %vw_hbm.1, bf16[32,2048]{1,0:T(8,128)(2,1)} %bitcast.5, bf16[64,2048]{1,0:T(8,128)(2,1)} %bitcast.3, ...), custom_call_target="tpu_custom_call" | custom-call | tf_op jit(solution)/shard_map/attend/pallas_call | solution.py:491
  16.5 0.8 %copy.13 = bf16[256,1024]{1,0:T(8,128)(2,1)} copy(bf16[256,1024]{1,0:T(8,128)(2,1)S(1)} %attend.1) | data formatting | bytes 1048576

commit v4 on v3

--- a/solution.py
+++ b/solution.py
@@ -74,6 +74,7 @@
     recv_z,
     send_y,
     recv_y,
+    send_w,
     send_s,
     recv_s,
     send_m,
@@ -225,7 +226,22 @@
         lax.fori_loop(jnp.minimum(z + 1, outer), jnp.minimum(z + 2, outer), z_send, 0)
 
     def send_far():
-        lax.fori_loop(jnp.minimum(z + 2, outer), outer, z_send, 0)
+        @pl.when(z == 0)
+        def _():
+            lax.fori_loop(min(2, outer), outer, z_send, 0)
+
+    def pass_on(source_z, part):
+        return pltpu.make_async_remote_copy(
+            src_ref=slot(source_z * inner + y, part),
+            dst_ref=slot(source_z * inner + y, part),
+            send_sem=send_w.at[source_z],
+            recv_sem=recv_z.at[source_z, part],
+            device_id={"kv": (z + 1) * inner + y},
+            device_id_type=MESH,
+        )
+
+    def passes(source_z):
+        return (source_z > 0) & (z < outer - 1)
 
     def send_across():
         if inner == 2:
@@ -321,11 +337,32 @@
                 low64, pltpu.roll(two, HEAD_DIM, 1), unit
             ).astype(BF16)
     send_at(3)
+    def forward(step, carry):
+        is_near = jnp.where((step == 1) | (g == 1), 1, 0)
+        source = is_near * (z - step) + (1 - is_near) * (step - 2)
+        for part in range(PARTS):
+            z_copy(source, z, part).wait_recv()
+
+            @pl.when(passes(source))
+            def _():
+                pass_on(source, part).start()
+
+            if inner == 2:
+                y_copy(source, y, part).start()
+        return carry
+
+    def first_forward():
+        lax.fori_loop(1, jnp.minimum(z, 1) + 1, forward, 0)
+
+    first_forward()
+
+
     gw_c.wait()
     gates = jax.nn.sigmoid(dot_t(tok[...], gw[...]))
     half = gates.shape[1] // 2
     gate_s = jnp.where(g == 0, gates[:, :heads], gates[:, heads:half])
     gate_c = jnp.where(g == 0, gates[:, half : half + heads], gates[:, half + heads :])
+    send_at(5)
     for b in range(blocks):
         rows = slice(b * BLOCK, (b + 1) * BLOCK)
         for h in range(heads):
@@ -334,6 +371,10 @@
             summary_mix[b, at] = jnp.broadcast_to(gate_s[rows, h : h + 1], (BLOCK, LANES))
 
     def sum_send(target, carry):
+        @pl.when((z > 0) & (target > z + 1))
+        def _():
+            pl.semaphore_wait(ready.at[target], 1)
+
         sum_copy(z, target).start()
         return carry
 
@@ -342,16 +383,7 @@
         sum_swap(yours).wait_recv()
     lax.fori_loop(z + 1, outer, sum_send, 0)
 
-    def forward(step, carry):
-        is_first = jnp.int32(step == 1)
-        source = is_first * (z - 1) + (1 - is_first) * (step - 2)
-        for part in range(PARTS):
-            z_copy(source, z, part).wait_recv()
-            if inner == 2:
-                y_copy(source, y, part).start()
-        return carry
-
-    lax.fori_loop(1, z + 1, forward, 0)
+    lax.fori_loop(2, z + 1, forward, 0)
 
     def sum_wait(source, carry):
         sum_copy(source, z).wait_recv()
@@ -455,7 +487,14 @@
         pltpu.make_async_copy(full(me), full(me), send_z.at[target]).wait()
         return carry
 
-    lax.fori_loop(z + 1, outer, z_done, 0)
+    last = jnp.where(z == 0, outer, jnp.minimum(z + 2, outer))
+    lax.fori_loop(z + 1, last, z_done, 0)
+
+    def pass_done(source, carry):
+        pltpu.make_async_copy(full(me), full(me), send_w.at[source]).wait()
+        return carry
+
+    lax.fori_loop(1, jnp.where(z < outer - 1, z, 1), pass_done, 0)
 
     def sum_done(target, carry):
         sum_copy(z, target).wait_send()
@@ -521,6 +560,7 @@
             dma((outer,)),
             dma((outer,)),
             dma((outer,)),
+            dma((outer,)),
             dma((1,)),
             dma((1,)),
         ],

time: 17.4 us -> 16.4 us (0.943)
  Pallas kernels: 16.5 us -> 15.5 us
    pallas_call x1, Pallas kernels: 16.5 us -> 15.5 us  [per_device(): pl.pallas_call(functools.partial(kernel, n_kv, inner), out_shape=pltpu.VM...]
where the time goes in v4:
time: 16.4 us; the launch traced here: 16.3 us
  Pallas kernels  15.5 us (95%)
  local copies, waits for them, and re-layouts  0.8 us (5%)
    pallas_call x1, Pallas kernels, per_device(): pl.pallas_call(functools.partial(kernel, n_kv, inner), out_shape=pltpu.VM...  15.5 us
    unnamed x1, local copies, waits for them, and re-layouts  0.8 us

profile of v4, /device:TPU:25, one launch (start us, length us, event | category | flops | bytes accessed | tf_op | source)
XLA Modules:
  0.0 16.3 jit_solution(8889957809902301768)
XLA Ops:
  0.0 15.5 %attend.1 = bf16[256,1024]{1,0:T(8,128)(2,1)S(1)} custom-call(s32[1,4,8]{2,1,0:T(4,128)} %sel_hbm.1, bf16[256,2048]{1,0:T(8,128)(2,1)} %tok_hbm.1, bf16[2048,512]{1,0:T(8,128)(2,1)} %qw_hbm.1, bf16[2048,128]{1,0:T(8,128)(2,1)} %kw_hbm.1, bf16[2048,128]{1,0:T(8,128)(2,1)} %vw_hbm.1, bf16[32,2048]{1,0:T(8,128)(2,1)} %bitcast.5, bf16[64,2048]{1,0:T(8,128)(2,1)} %bitcast.3, ...), custom_call_target="tpu_custom_call" | custom-call | tf_op jit(solution)/shard_map/attend/pallas_call | solution.py:530
  15.5 0.8 %copy.13 = bf16[256,1024]{1,0:T(8,128)(2,1)} copy(bf16[256,1024]{1,0:T(8,128)(2,1)S(1)} %attend.1) | data formatting | bytes 1048576

commit v5 on v4

--- a/solution.py
+++ b/solution.py
@@ -70,11 +70,9 @@
     partial,
     load_sem,
     ready,
-    send_z,
+    sent,
     recv_z,
-    send_y,
     recv_y,
-    send_w,
     send_s,
     recv_s,
     send_m,
@@ -200,7 +198,7 @@
         return pltpu.make_async_remote_copy(
             src_ref=slot(source_z * inner + y, part),
             dst_ref=slot(source_z * inner + y, part),
-            send_sem=send_z.at[target_z],
+            send_sem=sent.at[0],
             recv_sem=recv_z.at[source_z, part],
             device_id={"kv": target_z * inner + y},
             device_id_type=MESH,
@@ -210,7 +208,7 @@
         return pltpu.make_async_remote_copy(
             src_ref=slot(source_z * inner + source_y, part),
             dst_ref=slot(source_z * inner + source_y, part),
-            send_sem=send_y.at[source_z],
+            send_sem=sent.at[0],
             recv_sem=recv_y.at[source_z],
             device_id={"kv": z * inner + lax.rem(y + 1, inner)},
             device_id_type=MESH,
@@ -234,11 +232,27 @@
         return pltpu.make_async_remote_copy(
             src_ref=slot(source_z * inner + y, part),
             dst_ref=slot(source_z * inner + y, part),
-            send_sem=send_w.at[source_z],
+            send_sem=sent.at[0],
             recv_sem=recv_z.at[source_z, part],
             device_id={"kv": (z + 1) * inner + y},
             device_id_type=MESH,
         )
+
+    def pass_across(source_z, part):
+        return pltpu.make_async_remote_copy(
+            src_ref=slot(source_z * inner + y, part),
+            dst_ref=slot(source_z * inner + y, part),
+            send_sem=sent.at[0],
+            recv_sem=recv_y.at[source_z],
+            device_id={"kv": (z + 1) * inner},
+            device_id_type=MESH,
+        )
+
+    def crosses():
+        return (y == 1) & (g == 0) if inner == 2 else False
+
+    def handed_over(source_z):
+        return crosses() & (source_z > 0) & (source_z < z - 1)
 
     def passes(source_z):
         return (source_z > 0) & (z < outer - 1)
@@ -346,9 +360,18 @@
             @pl.when(passes(source))
             def _():
                 pass_on(source, part).start()
+                if inner == 2:
+
+                    @pl.when(crosses())
+                    def _():
+                        pass_across(source, part).start()
 
             if inner == 2:
-                y_copy(source, y, part).start()
+
+                @pl.when(jnp.logical_not(handed_over(source)))
+                def _():
+                    y_copy(source, y, part).start()
+
         return carry
 
     def first_forward():
@@ -462,7 +485,7 @@
             src_ref=own_mix.at[rows],
             dst_ref=peer_mix.at[rows],
             send_sem=send_m.at[0],
-            recv_sem=recv_m.at[0],
+            recv_sem=recv_m.at[2 * b // blocks],
             device_id={"tp": 1 - g},
             device_id_type=MESH,
         )
@@ -471,27 +494,29 @@
     own_rows = pl.ds(pl.multiple_of(g * cols, cols), cols)
     peer_rows = pl.ds(pl.multiple_of((1 - g) * cols, cols), cols)
     partial[...] = dot(own_mix[...], ow[own_rows, :])
-    all_mixes = pltpu.make_async_remote_copy(
-        src_ref=own_mix,
-        dst_ref=peer_mix,
-        send_sem=send_m.at[0],
-        recv_sem=recv_m.at[0],
-        device_id={"tp": 1 - g},
-        device_id_type=MESH,
-    )
-    all_mixes.wait_recv()
-    out_ref[...] = (partial[...] + dot(peer_mix[...], ow[peer_rows, :])).astype(BF16)
-    all_mixes.wait_send()
+    half_rows = local // 2
+    for part in range(2):
+        rows = slice(part * half_rows, (part + 1) * half_rows)
+        theirs = peer_mix.at[rows]
+        pltpu.make_async_copy(theirs, theirs, recv_m.at[part]).wait()
+        out_ref[rows] = (partial[rows] + dot(peer_mix[rows], ow[peer_rows, :])).astype(BF16)
+    pltpu.make_async_copy(own_mix, own_mix, send_m.at[0]).wait()
 
     def z_done(target, carry):
-        pltpu.make_async_copy(full(me), full(me), send_z.at[target]).wait()
+        pltpu.make_async_copy(full(me), full(me), sent.at[0]).wait()
         return carry
 
     last = jnp.where(z == 0, outer, jnp.minimum(z + 2, outer))
     lax.fori_loop(z + 1, last, z_done, 0)
 
     def pass_done(source, carry):
-        pltpu.make_async_copy(full(me), full(me), send_w.at[source]).wait()
+        pltpu.make_async_copy(full(me), full(me), sent.at[0]).wait()
+        if inner == 2:
+
+            @pl.when(crosses())
+            def _():
+                pltpu.make_async_copy(full(me), full(me), sent.at[0]).wait()
+
         return carry
 
     lax.fori_loop(1, jnp.where(z < outer - 1, z, 1), pass_done, 0)
@@ -505,7 +530,10 @@
         sum_swap(mine).wait_send()
 
         def y_done(step, carry):
-            pltpu.make_async_copy(full(me), full(me), send_y.at[z - step]).wait()
+            @pl.when(jnp.logical_not(handed_over(z - step)))
+            def _():
+                pltpu.make_async_copy(full(me), full(me), sent.at[0]).wait()
+
             return carry
 
         lax.fori_loop(y, z + 1, y_done, 0)
@@ -554,15 +582,13 @@
             vm((local, ow.shape[1]), F32),
             dma((CHUNKS + 8,)),
             pltpu.SemaphoreType.REGULAR((outer,)),
-            dma((outer,)),
+            dma((1,)),
             dma((outer, PARTS)),
             dma((outer,)),
             dma((outer,)),
             dma((outer,)),
-            dma((outer,)),
-            dma((outer,)),
             dma((1,)),
-            dma((1,)),
+            dma((2,)),
         ],
         compiler_params=pltpu.CompilerParams(
             collective_id=0, has_side_effects=True, vmem_limit_bytes=GRANT

time: 16.4 us -> 15.6 us (0.951)
  Pallas kernels: 15.5 us -> 14.7 us
    pallas_call x1, Pallas kernels: 15.5 us -> 14.7 us  [per_device(): pl.pallas_call(functools.partial(kernel, n_kv, inner), out_shape=pltpu.VM...]
where the time goes in v5:
time: 15.6 us; the launch traced here: 15.5 us
  Pallas kernels  14.7 us (94%)
  local copies, waits for them, and re-layouts  0.8 us (5%)
    pallas_call x1, Pallas kernels, per_device(): pl.pallas_call(functools.partial(kernel, n_kv, inner), out_shape=pltpu.VM...  14.7 us
    unnamed x1, local copies, waits for them, and re-layouts  0.8 us

profile of v5, /device:TPU:25, one launch (start us, length us, event | category | flops | bytes accessed | tf_op | source)
XLA Modules:
  0.0 15.5 jit_solution(1927664315276506062)
XLA Ops:
  0.0 14.7 %attend.1 = bf16[256,1024]{1,0:T(8,128)(2,1)S(1)} custom-call(s32[1,4,8]{2,1,0:T(4,128)} %sel_hbm.1, bf16[256,2048]{1,0:T(8,128)(2,1)} %tok_hbm.1, bf16[2048,512]{1,0:T(8,128)(2,1)} %qw_hbm.1, bf16[2048,128]{1,0:T(8,128)(2,1)} %kw_hbm.1, bf16[2048,128]{1,0:T(8,128)(2,1)} %vw_hbm.1, bf16[32,2048]{1,0:T(8,128)(2,1)} %bitcast.5, bf16[64,2048]{1,0:T(8,128)(2,1)} %bitcast.3, ...), custom_call_target="tpu_custom_call" | custom-call | tf_op jit(solution)/shard_map/attend/pallas_call | solution.py:558
  14.7 0.8 %copy.13 = bf16[256,1024]{1,0:T(8,128)(2,1)} copy(bf16[256,1024]{1,0:T(8,128)(2,1)S(1)} %attend.1) | data formatting | bytes 1048576

commit v6 on v5

--- a/solution.py
+++ b/solution.py
@@ -14,7 +14,8 @@
 MESH = pl.DeviceIdType.MESH
 F32 = jnp.float32
 BF16 = jnp.bfloat16
-CHUNKS = 4
+CUTS = (0, 4, 8, 12, 16)
+CHUNKS = len(CUTS) - 1
 PARTS = 4
 SEND_ORDER = ((0, 0, 1), (0, 0, 4))
 AHEAD = 8
@@ -112,10 +113,9 @@
 
     pl.semaphore_signal(barrier, inc=1, device_id={"tp": 1 - g}, device_id_type=MESH)
 
-    depth = width // CHUNKS
     first = []
     for c in range(CHUNKS):
-        part = pl.ds(c * depth, depth)
+        part = pl.ds(CUTS[c] * width // 16, (CUTS[c + 1] - CUTS[c]) * width // 16)
         trio = [
             pltpu.make_async_copy(tok_hbm.at[:, part], tok.at[:, part], load_sem.at[c]),
             pltpu.make_async_copy(
@@ -129,8 +129,6 @@
             copy.start()
         first.append(trio)
     base = CHUNKS
-    span_rows = depth * (local + 2 * LANES) // (2 * LANES)
-    whole_chunk = kvw.at[pl.ds(0, span_rows)]
     later = [
         pltpu.make_async_copy(src, dst, load_sem.at[base + i])
         for i, (src, dst) in enumerate(
@@ -166,14 +164,16 @@
 
     acc = jnp.zeros((local, 2 * LANES), F32)
     for c in range(CHUNKS):
-        pltpu.make_async_copy(whole_chunk, whole_chunk, load_sem.at[c]).wait()
+        depth = (CUTS[c + 1] - CUTS[c]) * width // 16
+        bulk = kvw.at[pl.ds(0, depth * (local + 2 * LANES) // (2 * LANES))]
+        pltpu.make_async_copy(bulk, bulk, load_sem.at[c]).wait()
         if c == 0:
             for copy in later[:4]:
                 copy.start()
         if c == CHUNKS - 2:
             for copy in later[4:]:
                 copy.start()
-        part = pl.ds(c * depth, depth)
+        part = pl.ds(CUTS[c] * width // 16, (CUTS[c + 1] - CUTS[c]) * width // 16)
         acc += dot(tok[:, part], kvw[part, :])
     keys = acc[:, :LANES]
     values = acc[:, LANES:]
@@ -310,7 +310,7 @@
         return pltpu.make_async_remote_copy(
             src_ref=sums.at[slot, :],
             dst_ref=sums.at[slot, :],
-            send_sem=send_s.at[z],
+            send_sem=send_s.at[0],
             recv_sem=recv_s.at[z],
             device_id=partner(),
             device_id_type=MESH,
@@ -325,7 +325,7 @@
         return pltpu.make_async_remote_copy(
             src_ref=slot,
             dst_ref=slot,
-            send_sem=send_s.at[target],
+            send_sem=send_s.at[0],
             recv_sem=recv_s.at[source],
             device_id={"kv": target * inner + y},
             device_id_type=MESH,
@@ -374,8 +374,10 @@
 
         return carry
 
+    early = jnp.where((g == 0) & (z < outer - 1), 2, 1)
+
     def first_forward():
-        lax.fori_loop(1, jnp.minimum(z, 1) + 1, forward, 0)
+        lax.fori_loop(1, jnp.minimum(z, early) + 1, forward, 0)
 
     first_forward()
 
@@ -406,7 +408,7 @@
         sum_swap(yours).wait_recv()
     lax.fori_loop(z + 1, outer, sum_send, 0)
 
-    lax.fori_loop(2, z + 1, forward, 0)
+    lax.fori_loop(early + 1, z + 1, forward, 0)
 
     def sum_wait(source, carry):
         sum_copy(source, z).wait_recv()
@@ -585,7 +587,7 @@
             dma((1,)),
             dma((outer, PARTS)),
             dma((outer,)),
-            dma((outer,)),
+            dma((1,)),
             dma((outer,)),
             dma((1,)),
             dma((2,)),

time: 15.6 us -> 15.6 us (level)
  no operation moved by 1% of the time
where the time goes in v6:
time: 15.6 us; the launch traced here: 15.5 us
  Pallas kernels  14.6 us (94%)
  local copies, waits for them, and re-layouts  0.8 us (5%)
    pallas_call x1, Pallas kernels, per_device(): pl.pallas_call(functools.partial(kernel, n_kv, inner), out_shape=pltpu.VM...  14.6 us
    unnamed x1, local copies, waits for them, and re-layouts  0.8 us

profile of v6, /device:TPU:25, one launch (start us, length us, event | category | flops | bytes accessed | tf_op | source)
XLA Modules:
  0.0 15.5 jit_solution(11674948685558776510)
XLA Ops:
  0.0 14.6 %attend.1 = bf16[256,1024]{1,0:T(8,128)(2,1)S(1)} custom-call(s32[1,4,8]{2,1,0:T(4,128)} %sel_hbm.1, bf16[256,2048]{1,0:T(8,128)(2,1)} %tok_hbm.1, bf16[2048,512]{1,0:T(8,128)(2,1)} %qw_hbm.1, bf16[2048,128]{1,0:T(8,128)(2,1)} %kw_hbm.1, bf16[2048,128]{1,0:T(8,128)(2,1)} %vw_hbm.1, bf16[32,2048]{1,0:T(8,128)(2,1)} %bitcast.5, bf16[64,2048]{1,0:T(8,128)(2,1)} %bitcast.3, ...), custom_call_target="tpu_custom_call" | custom-call | tf_op jit(solution)/shard_map/attend/pallas_call | solution.py:560
  14.7 0.8 %copy.13 = bf16[256,1024]{1,0:T(8,128)(2,1)} copy(bf16[256,1024]{1,0:T(8,128)(2,1)S(1)} %attend.1) | data formatting | bytes 1048576
